TPU v7x, 256 devices: a 4x2x16 block of a 4x16x16 slice. The times are simulated.
256 devices in a mesh: grp: 2 (over y), sp: 16 (over z), tp: 8 (over x, core).
Axes of the slice: x: 4, y: 2, z: 16, core: 2. Of those that a mesh axis runs over, the one named last changes fastest.
The devices are a block of a 4x16x16 slice.
Arguments:
- tokens: bfloat16 [32, 4096, 4096], P(('grp', 'tp'), 'sp'), parts along dimension 0, may hold values from -8 to 8, as said below
- offsets: int32 [32], P(('grp', 'tp')), parts along dimension 0, may hold values from 0 to 4095
- in_gain: float32 [4096], replicated, may hold values from 0.1 to 1.9
- w_latent: bfloat16 [4096, 1024], P('sp'), may hold values from -0.09375 to 0.09375
- w_rope_key: bfloat16 [4096, 32], replicated, may hold values from -0.09375 to 0.09375
- kv_gain: float32 [1024], replicated, may hold values from 0.1 to 1.9
- w_up_key: bfloat16 [1024, 2048], P(None, 'tp'), may hold values from -0.1875 to 0.1875
- w_up_value: bfloat16 [1024, 2048], P(None, 'tp'), may hold values from -0.1875 to 0.1875
- q_nope: bfloat16 [32, 2048], P(('grp', 'sp'), 'tp'), parts along dimension 0, may hold values from -300 to 300, as said below
- q_rope: bfloat16 [32, 1024], P(('grp', 'sp'), 'tp'), parts along dimension 0, may hold values from -16 to 16
Outputs:
- keys: bfloat16 [32, 4096, 2048], P(('grp', 'sp'), None, 'tp'), parts along dimension 0
- values: bfloat16 [32, 4096, 2048], P(('grp', 'sp'), None, 'tp'), parts along dimension 0
- rope_keys: bfloat16 [32, 32, 4096], P(('grp', 'sp')), parts along dimension 0
- read: bfloat16 [32, 2048], P(('grp', 'sp'), 'tp'), parts along dimension 0
There are 2 independent parts, one for each index of `grp`. A program takes and returns all parts, laid end to end along the dimension named above; an argument that names none is the same for every part. Nothing has to cross between parts.
Inputs may be any that keep to these rules, and one draw needn't show every extreme that they name: `tokens`: entries of the layer's input. `q_nope`: entries of the first decoding token's queries.
All inputs are finite; a program needn't handle non-finite values.
Results may differ from a plain program's by a relative error of at most 0.02.
Values may be sent and summed in bfloat16 or wider, within the bound.
A program may use at most 128 MiB of HBM per device.

v0:
```python
import jax
import jax.numpy as jnp
from jax import lax
from jax.sharding import PartitionSpec as P

HEAD = 64
ROPE = 32
EPS = 1e-06


def joined_along(tiles, dim):
    shape = list(tiles.shape[1:])
    shape[dim] *= tiles.shape[0]
    return jnp.moveaxis(tiles, 0, dim).reshape(shape)


def copy_for_each(value, axis):
    peers = lax.axis_size(axis)
    return lax.all_to_all(
        jnp.broadcast_to(value[None], (peers, *value.shape)), axis, 0, 0, tiled=True
    )


def gather_directly(value, axis, dim):
    return joined_along(copy_for_each(value, axis), dim)


def rms_scale(values, gain):
    wide = values.astype(jnp.float32)
    return wide * lax.rsqrt(jnp.mean(wide * wide, axis=-1, keepdims=True) + EPS) * gain


def rotate(raw, position):
    inverse = 10000.0 ** (-jnp.arange(0, ROPE, 2).astype(jnp.float32) / ROPE)
    angle = position.astype(jnp.float32)[..., None] * inverse
    cosine, sine = (jnp.cos(angle), jnp.sin(angle))
    half = ROPE // 2
    first, second = (raw[..., :half], raw[..., half:])
    return jnp.concatenate(
        [first * cosine - second * sine, second * cosine + first * sine], axis=-1
    )


def local(
    tokens, offsets, in_gain, w_latent, w_rope_key, kv_gain, w_up_key, w_up_value, q_nope, q_rope
):
    prompts, rows, width = tokens.shape
    n_sp = lax.axis_size("sp")
    length = n_sp * rows
    block = lax.axis_index("sp")
    normed = rms_scale(tokens.reshape(prompts * rows, width), in_gain).astype(jnp.bfloat16)
    latent_raw = jnp.dot(
        normed,
        lax.all_gather(w_latent, "sp", axis=0, tiled=True),
        preferred_element_type=jnp.float32,
    )
    latent = rms_scale(latent_raw, kv_gain).astype(jnp.bfloat16)
    position = offsets[:, None] + block * rows + jnp.arange(rows, dtype=jnp.int32)[None, :]
    rope_raw = jnp.dot(normed, w_rope_key, preferred_element_type=jnp.float32).reshape(
        prompts, rows, ROPE
    )
    rotated = rotate(rope_raw, position).astype(jnp.bfloat16)
    head_cols = w_up_key.shape[1]
    paired = jnp.stack([w_up_key, w_up_value])
    both = jnp.einsum(
        "tk,skc->stc",
        latent,
        lax.all_gather(paired, "tp", axis=2, tiled=True),
        preferred_element_type=jnp.float32,
    ).astype(jnp.bfloat16)
    both = both.reshape(2, prompts, rows, both.shape[2])
    by_head = lax.all_to_all(both, "tp", split_axis=3, concat_axis=1, tiled=True)
    rope_every = gather_directly(rotated, "tp", 0)
    moved, rope_moved = (
        lax.all_to_all(by_head[:, :, None], "sp", split_axis=1, concat_axis=2, tiled=True),
        lax.all_to_all(rope_every[None, :, None], "sp", split_axis=1, concat_axis=2, tiled=True),
    )
    keys = moved[0].reshape(length, head_cols)
    values = moved[1].reshape(length, head_cols)
    rope_all = rope_moved.reshape(length, ROPE)
    rope_keys = rope_all.T
    heads_here = head_cols // HEAD
    query = q_nope.reshape(heads_here, HEAD)
    rotary_q = q_rope.reshape(heads_here, ROPE)
    keys_split = keys.reshape(length, heads_here, HEAD)
    scores = jnp.einsum("hd,jhd->hj", query, keys_split, preferred_element_type=jnp.float32)
    scores = scores + jnp.dot(rotary_q, rope_keys, preferred_element_type=jnp.float32)
    scores = scores / jnp.sqrt(jnp.float32(HEAD + ROPE))
    peak = jnp.max(scores, axis=-1, keepdims=True)
    expo = jnp.exp(scores - peak)
    weights = (expo / jnp.sum(expo, axis=-1, keepdims=True)).astype(jnp.bfloat16)
    read = jnp.einsum(
        "hj,jhd->hd",
        weights,
        values.reshape(length, heads_here, HEAD),
        preferred_element_type=jnp.float32,
    )
    read = read.astype(jnp.bfloat16).reshape(1, heads_here * HEAD)
    return (keys[None], values[None], rope_keys[None], read)


def solution(mesh):
    in_specs = (
        P(("grp", "tp"), "sp", None),
        P(("grp", "tp")),
        P(),
        P("sp", None),
        P(),
        P(),
        P(None, "tp"),
        P(None, "tp"),
        P(("grp", "sp"), "tp"),
        P(("grp", "sp"), "tp"),
    )
    out_specs = (
        P(("grp", "sp"), None, "tp"),
        P(("grp", "sp"), None, "tp"),
        P(("grp", "sp"), None, None),
        P(("grp", "sp"), "tp"),
    )
    return jax.shard_map(local, mesh=mesh, in_specs=in_specs, out_specs=out_specs, check_vma=False)
```

profile of v0, /device:TPU:33, one launch (start us, length us, event | category | flops | bytes accessed | tf_op | source)
XLA Modules:
  0.0 515.6 jit_solution(11231751343885072324)
XLA Ops:
  8.1 2.3 pad_maximum_fusion
  11.3 3.3 multiply_reduce_fusion
  17.2 23.7 %all-to-all-start.2 = ((bf16[8,2,256,32]{2,1,3,0:T(2,128)(2,1)}), bf16[8,2,256,32]{2,1,3,0:T(2,128)(2,1)S(1)}, u32[]{:S(2)}, u32[]{:S(2)}) async-start(bf16[8,2,256,32]{2,1,3,0:T(2,128)(2,1)} %broadcast_in_dim.7), calls=%async_computation.2 | async-start | bytes 524288 | tf_op jit(solution)/shard_map/all_to_all | solution.py:19
  40.9 5.8 %fusion.1 = bf16[512,4096]{1,0:T(8,128)(2,1)} fusion(bf16[2,256,4096]{2,1,0:T(8,128)(2,1)} %param.10, f32[4096]{0:T(1024)S(1)} %copy-done.6, f32[512]{0:T(512)S(1)} %bitcast.76), kind=kLoop, calls=%fused_computation.2 | loop fusion | flops 8388608 | bytes 8407040 | tf_op jit(solution)/shard_map/convert_element_type | solution.py:51
  46.7 81.6 %all-gather.5.cloned.1.call-done = bf16[4096,1024]{1,0:T(8,128)(2,1)} async-done(((bf16[256,1024]{1,0:T(8,128)(2,1)}), bf16[4096,1024]{1,0:T(8,128)(2,1)}) %all-gather.5.cloned.1.call-update) | async-done | bytes 8388624 | tf_op jit(solution)/shard_map/all_gather | solution.py:54
  128.3 8.3 %multiply_reduce_fusion.1 = (f32[512]{0:T(512)S(1)}, f32[512,1024]{1,0:T(8,128)S(1)}) fusion(bf16[512,4096]{1,0:T(8,128)(2,1)} %fusion.1, bf16[4096,1024]{1,0:T(8,128)(2,1)} %all-gather.5.cloned.1.call-done), kind=kOutput, calls=%fused_computation.14 | convolution fusion | flops 4296015360 | bytes 14682112 | tf_op jit(solution)/shard_map/dot_general | solution.py:52
  136.6 52.3 %all-gather.3.cloned.1.call-done = bf16[2,1024,2048]{2,1,0:T(8,128)(2,1)} async-done(((bf16[2,1024,256]{2,1,0:T(8,128)(2,1)}), bf16[2,1024,2048]{2,1,0:T(8,128)(2,1)}) %all-gather.3.cloned.1.call-update) | async-done | bytes 8388624 | tf_op jit(solution)/shard_map/all_gather | solution.py:68
  188.9 9.6 %convolution_convert_fusion = bf16[2,2048,512]{1,2,0:T(8,128)(2,1)} fusion(bf16[2,1024,2048]{2,1,0:T(8,128)(2,1)} %all-gather.3.cloned.1.call-done, f32[512,1024]{1,0:T(8,128)S(1)} %get-tuple-element.11, f32[1024]{0:T(1024)S(1)} %copy-done.8, f32[512]{0:T(512)S(1)} %add_rsqrt_fusion), kind=kOutput, calls=%fused_computation.12 | convolution fusion | flops 4298637312 | bytes 14686208 | tf_op jit(solution)/shard_map/tk,skc->stc/dot_general | solution.py:65
  198.6 11.2 %copy.25 = bf16[2,2,256,2048]{2,1,0,3:T(2,128)(2,1)} copy(bf16[2,2,256,2048]{3,2,1,0:T(8,128)(2,1)} %bitcast.68) | data formatting | bytes 8388608 | tf_op jit(solution)/shard_map/reshape | solution.py:71
  209.8 4.7 all-to-all-start
  215.2 48.1 %all-to-all-done = bf16[2,2,256,2048]{2,1,0,3:T(2,128)(2,1)} async-done(((bf16[2,2,256,2048]{2,1,0,3:T(2,128)(2,1)}), bf16[2,2,256,2048]{2,1,0,3:T(2,128)(2,1)}, u32[]{:S(2)}, u32[]{:S(2)}) %all-to-all-start) | async-done | bytes 4194336 | tf_op jit(solution)/shard_map/all_to_all | solution.py:72
  263.3 12.1 %all-to-all-start.3 = ((bf16[1,16,1,256,32]{3,4,2,0,1:T(8,128)(2,1)}), bf16[1,16,1,256,32]{3,4,2,0,1:T(8,128)(2,1)S(1)}, u32[]{:S(2)}, u32[]{:S(2)}) async-start(bf16[1,16,1,256,32]{3,4,2,0,1:T(8,128)(2,1)} %bitcast.13), calls=%async_computation.3 | async-start | bytes 524288 | tf_op jit(solution)/shard_map/all_to_all | solution.py:76
  275.4 4.9 copy.26
  280.4 7.7 %all-to-all-done.3 = bf16[1,16,1,256,32]{3,4,2,0,1:T(8,128)(2,1)S(1)} async-done(((bf16[1,16,1,256,32]{3,4,2,0,1:T(8,128)(2,1)}), bf16[1,16,1,256,32]{3,4,2,0,1:T(8,128)(2,1)S(1)}, u32[]{:S(2)}, u32[]{:S(2)}) %all-to-all-start.3) | async-done | bytes 262176 | tf_op jit(solution)/shard_map/all_to_all | solution.py:76
  288.1 11.6 %all-to-all-start.1 = ((bf16[2,16,1,256,256]{3,4,2,0,1:T(8,128)(2,1)}), bf16[2,16,1,256,256]{3,4,2,0,1:T(8,128)(2,1)}, u32[]{:S(2)}, u32[]{:S(2)}) async-start(bf16[2,16,1,256,256]{3,4,2,0,1:T(8,128)(2,1)} %bitcast.67), calls=%async_computation.1 | async-start | bytes 8388608 | tf_op jit(solution)/shard_map/all_to_all | solution.py:75
  301.1 180.2 %all-to-all-done.1 = bf16[2,16,1,256,256]{3,4,2,0,1:T(8,128)(2,1)} async-done(((bf16[2,16,1,256,256]{3,4,2,0,1:T(8,128)(2,1)}), bf16[2,16,1,256,256]{3,4,2,0,1:T(8,128)(2,1)}, u32[]{:S(2)}, u32[]{:S(2)}) %all-to-all-start.1) | async-done | bytes 4194336 | tf_op jit(solution)/shard_map/all_to_all | solution.py:75
  481.3 2.6 fusion.26
  485.2 2.5 copy.34
  487.8 3.9 copy.40
  491.7 2.5 copy.33
  494.2 2.4 copy.39
  496.5 4.3 reshape_reshape_squeeze.6
  503.5 2.3 reshape_reshape_squeeze.7
  505.8 2.2 fusion.13
  (49 shorter events, 11.1 us)
Async XLA Ops:
  7.2 7.4 %copy-start = (bf16[4096,32]{0,1:T(8,128)(2,1)S(1)}, bf16[4096,32]{0,1:T(8,128)(2,1)}, u32[]{:S(2)}) copy-start(bf16[4096,32]{0,1:T(8,128)(2,1)} %param.14) | copy-start | bytes 786436
  7.2 7.4 %copy-start.6 = (f32[4096]{0:T(1024)S(1)}, f32[4096]{0:T(1024)}, u32[]{:S(2)}) copy-start(f32[4096]{0:T(1024)} %param.12) | copy-start | bytes 49156
  7.2 121.1 %all-gather.5.cloned.1.call-start = ((), (), s32[]{:S(2)}) async-start(), calls=%async_computation.5 | async-start | bytes 8912896 | tf_op jit(solution)/shard_map/all_gather | solution.py:54
  8.0 180.9 %all-gather.3.cloned.1.call-start = ((), (), s32[]{:S(2)}) async-start(), calls=%async_computation.4 | async-start | bytes 9437184 | tf_op jit(solution)/shard_map/all_gather | solution.py:68
  10.4 4.2 copy-start.3
  17.2 192.6 %all-to-all-start.2 = ((bf16[8,2,256,32]{2,1,3,0:T(2,128)(2,1)}), bf16[8,2,256,32]{2,1,3,0:T(2,128)(2,1)S(1)}, u32[]{:S(2)}, u32[]{:S(2)}) async-start(bf16[8,2,256,32]{2,1,3,0:T(2,128)(2,1)} %broadcast_in_dim.7), calls=%async_computation.2 | async-start | bytes 524288 | tf_op jit(solution)/shard_map/all_to_all | solution.py:19
  46.7 142.2 %copy-start.8 = (f32[1024]{0:T(1024)S(1)}, f32[1024]{0:T(1024)}, u32[]{:S(2)}) copy-start(f32[1024]{0:T(1024)} %param.15) | copy-start | bytes 12292
  209.8 53.6 %all-to-all-start = ((bf16[2,2,256,2048]{2,1,0,3:T(2,128)(2,1)}), bf16[2,2,256,2048]{2,1,0,3:T(2,128)(2,1)}, u32[]{:S(2)}, u32[]{:S(2)}) async-start(bf16[2,2,256,2048]{2,1,0,3:T(2,128)(2,1)} %copy.25), calls=%async_computation | async-start | bytes 8388608 | tf_op jit(solution)/shard_map/all_to_all | solution.py:72
  263.3 24.8 %all-to-all-start.3 = ((bf16[1,16,1,256,32]{3,4,2,0,1:T(8,128)(2,1)}), bf16[1,16,1,256,32]{3,4,2,0,1:T(8,128)(2,1)S(1)}, u32[]{:S(2)}, u32[]{:S(2)}) async-start(bf16[1,16,1,256,32]{3,4,2,0,1:T(8,128)(2,1)} %bitcast.13), calls=%async_computation.3 | async-start | bytes 524288 | tf_op jit(solution)/shard_map/all_to_all | solution.py:76
  288.1 11.6 %copy-start.7 = (bf16[1,256]{1,0:T(2,128)(2,1)S(1)}, bf16[1,256]{1,0:T(2,128)(2,1)}, u32[]{:S(2)}) copy-start(bf16[1,256]{1,0:T(2,128)(2,1)} %param.18) | copy-start | bytes 1540
  288.1 12.2 %copy-start.9 = (bf16[1,128]{1,0:T(2,128)(2,1)S(1)}, bf16[1,128]{1,0:T(2,128)(2,1)}, u32[]{:S(2)}) copy-start(bf16[1,128]{1,0:T(2,128)(2,1)} %param.19) | copy-start | bytes 772
  288.1 193.2 %all-to-all-start.1 = ((bf16[2,16,1,256,256]{3,4,2,0,1:T(8,128)(2,1)}), bf16[2,16,1,256,256]{3,4,2,0,1:T(8,128)(2,1)}, u32[]{:S(2)}, u32[]{:S(2)}) async-start(bf16[2,16,1,256,256]{3,4,2,0,1:T(8,128)(2,1)} %bitcast.67), calls=%async_computation.1 | async-start | bytes 8388608 | tf_op jit(solution)/shard_map/all_to_all | solution.py:75
  301.1 201.8 %copy-start.5 = (bf16[4,8,16,256]{3,1,2,0:T(8,128)(2,1)}, bf16[4,8,16,256]{3,1,2,0:T(8,128)(2,1)S(1)}, u32[]{:S(2)}) copy-start(bf16[4,8,16,256]{3,1,2,0:T(8,128)(2,1)S(1)} %copy.44) | copy-start | bytes 786436
  483.9 1.3 copy-start.2
  496.5 6.9 %copy-start.4 = (bf16[1,16,1,256,256]{3,1,4,2,0:T(8,128)(2,1)S(1)}, bf16[1,16,1,256,256]{3,1,4,2,0:T(8,128)(2,1)}, u32[]{:S(2)}) copy-start(bf16[1,16,1,256,256]{3,1,4,2,0:T(8,128)(2,1)} %copy.34) | copy-start | bytes 6291460
  496.5 12.2 %copy-start.1 = (bf16[4096,32]{0,1:T(8,128)(2,1)S(1)}, bf16[4096,32]{0,1:T(8,128)(2,1)}, u32[]{:S(2)}) copy-start(bf16[4096,32]{0,1:T(8,128)(2,1)} %param.14) | copy-start | bytes 786436
Sparse Core Ops, SparseCore 0:
  9.8 118.4 all-gather.4
  130.7 58.1 all-gather.2
where the time goes:
time: 517 us; the launch traced here: 516 us
  waiting for transfers between devices  371 us (72%)
  starting transfers between devices  52.2 us (10%)
  local copies, waits for them, and re-layouts  41 us (8%)
  matrix products  23.8 us (5%)
  between operations  14.2 us (3%)
  other arithmetic  13.5 us (3%)
    all_to_all x1, waiting for transfers between devices, local(): lax.all_to_all(by_head[:, :, None], 'sp', split_axis=1, concat_axis=2, ti...  180 us
    all_gather x1, waiting for transfers between devices, local(): lax.all_gather(w_latent, 'sp', axis=0, tiled=True)  81.6 us
    all_gather x1, waiting for transfers between devices, local(): lax.all_gather(paired, 'tp', axis=2, tiled=True)  52.3 us
    all_to_all x1, waiting for transfers between devices, local(): lax.all_to_all(both, 'tp', split_axis=3, concat_axis=1, tiled=True)  48.1 us
    all_to_all x1, starting transfers between devices, copy_for_each(): lax.all_to_all(jnp.broadcast_to(value[None], (peers, *value.shape)), axis...  23.7 us
    all_to_all x1, starting transfers between devices, local(): lax.all_to_all(rope_every[None, :, None], 'sp', split_axis=1, concat_axis...  12.1 us
    all_to_all x1, starting transfers between devices, local(): lax.all_to_all(by_head[:, :, None], 'sp', split_axis=1, concat_axis=2, ti...  11.6 us
    reshape x1, local copies, waits for them, and re-layouts, local(): both = both.reshape(2, prompts, rows, both.shape[2])  11.2 us
  transfers between devices with their start and end apart: 6, of which 5 were waited for; matrix products, arithmetic and copies ran while one was open for 10% of the time, Pallas kernels for 0%

commit v1 on v0

--- a/solution.py
+++ b/solution.py
@@ -69,7 +69,9 @@
         preferred_element_type=jnp.float32,
     ).astype(jnp.bfloat16)
     both = both.reshape(2, prompts, rows, both.shape[2])
-    by_head = lax.all_to_all(both, "tp", split_axis=3, concat_axis=1, tiled=True)
+    by_head = jnp.concatenate(
+        lax.all_to_all(jnp.stack(jnp.split(both, lax.axis_size("tp"), axis=3)), "tp", 0, 0), axis=1
+    )
     rope_every = gather_directly(rotated, "tp", 0)
     moved, rope_moved = (
         lax.all_to_all(by_head[:, :, None], "sp", split_axis=1, concat_axis=2, tiled=True),

time: 517 us -> 504 us (0.975)
  local copies, waits for them, and re-layouts: 41 us -> 31.8 us
    reshape x1 -> x0, local copies, waits for them, and re-layouts: 11.2 us -> none  [local(): both = both.reshape(2, prompts, rows, both.shape[2])]
  transfers between devices with their start and end apart: 6 -> 6, of which waited for: 5 -> 5; matrix products, arithmetic and copies ran while one was open for 10% -> 9% of each run, Pallas kernels for 0% -> 0%
where the time goes in v1:
time: 504 us
  waiting for transfers between devices  371 us (74%)
  starting transfers between devices  52.1 us (10%)
  local copies, waits for them, and re-layouts  31.8 us (6%)
  matrix products  20.9 us (4%)
  between operations  14.3 us (3%)
  other arithmetic  13.5 us (3%)
    all_to_all x1, waiting for transfers between devices, local(): lax.all_to_all(by_head[:, :, None], 'sp', split_axis=1, concat_axis=2, ti...  180 us
    all_gather x1, waiting for transfers between devices, local(): lax.all_gather(w_latent, 'sp', axis=0, tiled=True)  81.6 us
    all_gather x1, waiting for transfers between devices, local(): lax.all_gather(paired, 'tp', axis=2, tiled=True)  52.3 us
    all_to_all x1, waiting for transfers between devices, local(): lax.all_to_all(jnp.stack(jnp.split(both, lax.axis_size('tp'), axis=3)), '...  48.1 us
    all_to_all x1, starting transfers between devices, copy_for_each(): lax.all_to_all(jnp.broadcast_to(value[None], (peers, *value.shape)), axis...  23.7 us
    all_to_all x1, starting transfers between devices, local(): lax.all_to_all(rope_every[None, :, None], 'sp', split_axis=1, concat_axis...  12.1 us
    all_to_all x1, starting transfers between devices, local(): lax.all_to_all(by_head[:, :, None], 'sp', split_axis=1, concat_axis=2, ti...  11.4 us
  transfers between devices with their start and end apart: 6, of which 5 were waited for; matrix products, arithmetic and copies ran while one was open for 9% of the time, Pallas kernels for 0%

profile of v1, /device:TPU:33, one launch (start us, length us, event | category | flops | bytes accessed | tf_op | source)
XLA Modules:
  0.0 503.5 jit_solution(15954407040946968766)
XLA Ops:
  8.1 2.3 pad_maximum_fusion
  11.3 3.3 multiply_reduce_fusion
  14.7 1.4 fusion.4
  17.2 23.7 %all-to-all-start.2 = ((bf16[8,2,256,32]{2,1,3,0:T(2,128)(2,1)}), bf16[8,2,256,32]{2,1,3,0:T(2,128)(2,1)S(1)}, u32[]{:S(2)}, u32[]{:S(2)}) async-start(bf16[8,2,256,32]{2,1,3,0:T(2,128)(2,1)} %broadcast_in_dim.4), calls=%async_computation.2 | async-start | bytes 524288 | tf_op jit(solution)/shard_map/all_to_all | solution.py:19
  40.9 5.8 %fusion.1 = bf16[512,4096]{1,0:T(8,128)(2,1)} fusion(bf16[2,256,4096]{2,1,0:T(8,128)(2,1)} %param.10, f32[4096]{0:T(1024)S(1)} %copy-done.5, f32[512]{0:T(512)S(1)} %bitcast.114), kind=kLoop, calls=%fused_computation.2 | loop fusion | flops 8388608 | bytes 8407040 | tf_op jit(solution)/shard_map/convert_element_type | solution.py:51
  46.7 81.6 %all-gather.5.cloned.1.call-done = bf16[4096,1024]{1,0:T(8,128)(2,1)} async-done(((bf16[256,1024]{1,0:T(8,128)(2,1)}), bf16[4096,1024]{1,0:T(8,128)(2,1)}) %all-gather.5.cloned.1.call-update) | async-done | bytes 8388624 | tf_op jit(solution)/shard_map/all_gather | solution.py:54
  128.3 8.3 %multiply_reduce_fusion.1 = (f32[512]{0:T(512)S(1)}, f32[512,1024]{1,0:T(8,128)S(1)}) fusion(bf16[512,4096]{1,0:T(8,128)(2,1)} %fusion.1, bf16[4096,1024]{1,0:T(8,128)(2,1)} %all-gather.5.cloned.1.call-done), kind=kOutput, calls=%fused_computation.14 | convolution fusion | flops 4296015360 | bytes 14682112 | tf_op jit(solution)/shard_map/dot_general | solution.py:52
  136.6 52.3 %all-gather.3.cloned.1.call-done = bf16[2,1024,2048]{2,1,0:T(8,128)(2,1)} async-done(((bf16[2,1024,256]{2,1,0:T(8,128)(2,1)}), bf16[2,1024,2048]{2,1,0:T(8,128)(2,1)}) %all-gather.3.cloned.1.call-update) | async-done | bytes 8388624 | tf_op jit(solution)/shard_map/all_gather | solution.py:68
  188.9 8.3 %convolution_convert_fusion = bf16[2,2048,512]{1,2,0:T(8,128)(2,1)S(1)} fusion(bf16[2,1024,2048]{2,1,0:T(8,128)(2,1)} %all-gather.3.cloned.1.call-done, f32[512,1024]{1,0:T(8,128)S(1)} %get-tuple-element.11, f32[1024]{0:T(1024)S(1)} %copy-done.7, f32[512]{0:T(512)S(1)} %add_rsqrt_fusion), kind=kOutput, calls=%fused_computation.12 | convolution fusion | flops 4298637312 | bytes 14686208 | tf_op jit(solution)/shard_map/tk,skc->stc/dot_general | solution.py:65
  204.4 4.7 all-to-all-start
  209.8 48.1 %all-to-all-done = bf16[8,2,2,256,256]{4,3,2,1,0:T(8,128)(2,1)} async-done(((bf16[8,2,2,256,256]{4,3,2,1,0:T(8,128)(2,1)}), bf16[8,2,2,256,256]{4,3,2,1,0:T(8,128)(2,1)}, u32[]{:S(2)}, u32[]{:S(2)}) %all-to-all-start) | async-done | bytes 4194336 | tf_op jit(solution)/shard_map/all_to_all | solution.py:73
  257.9 12.1 %all-to-all-start.3 = ((bf16[1,16,1,256,32]{3,4,2,0,1:T(8,128)(2,1)}), bf16[1,16,1,256,32]{3,4,2,0,1:T(8,128)(2,1)S(1)}, u32[]{:S(2)}, u32[]{:S(2)}) async-start(bf16[1,16,1,256,32]{3,4,2,0,1:T(8,128)(2,1)} %bitcast.21), calls=%async_computation.3 | async-start | bytes 524288 | tf_op jit(solution)/shard_map/all_to_all | solution.py:78
  270.0 2.5 copy.30
  272.5 2.2 copy.31
  274.7 8.0 %all-to-all-done.3 = bf16[1,16,1,256,32]{3,4,2,0,1:T(8,128)(2,1)S(1)} async-done(((bf16[1,16,1,256,32]{3,4,2,0,1:T(8,128)(2,1)}), bf16[1,16,1,256,32]{3,4,2,0,1:T(8,128)(2,1)S(1)}, u32[]{:S(2)}, u32[]{:S(2)}) %all-to-all-start.3) | async-done | bytes 262176 | tf_op jit(solution)/shard_map/all_to_all | solution.py:78
  282.7 11.4 %all-to-all-start.1 = ((bf16[2,16,1,256,256]{4,3,0,2,1:T(8,128)(2,1)}), bf16[2,16,1,256,256]{4,3,0,2,1:T(8,128)(2,1)}, u32[]{:S(2)}, u32[]{:S(2)}) async-start(bf16[2,16,1,256,256]{4,3,0,2,1:T(8,128)(2,1)} %copy.31), calls=%async_computation.1 | async-start | bytes 8388608 | tf_op jit(solution)/shard_map/all_to_all | solution.py:77
  295.6 180.2 %all-to-all-done.1 = bf16[2,16,1,256,256]{4,3,0,2,1:T(8,128)(2,1)} async-done(((bf16[2,16,1,256,256]{4,3,0,2,1:T(8,128)(2,1)}), bf16[2,16,1,256,256]{4,3,0,2,1:T(8,128)(2,1)}, u32[]{:S(2)}, u32[]{:S(2)}) %all-to-all-start.1) | async-done | bytes 4194336 | tf_op jit(solution)/shard_map/all_to_all | solution.py:77
  475.8 3.9 fusion.34
  479.7 1.3 copy-done.3
  481.0 3.1 copy.36
  484.1 2.9 reshape_reshape_squeeze.6
  488.0 3.4 copy.37
  491.4 2.3 reshape_reshape_squeeze.7
  493.8 2.2 fusion.21
  (53 shorter events, 13.8 us)
Async XLA Ops:
  7.2 7.4 %copy-start = (bf16[4096,32]{0,1:T(8,128)(2,1)S(1)}, bf16[4096,32]{0,1:T(8,128)(2,1)}, u32[]{:S(2)}) copy-start(bf16[4096,32]{0,1:T(8,128)(2,1)} %param.14) | copy-start | bytes 786436
  7.2 7.4 %copy-start.5 = (f32[4096]{0:T(1024)S(1)}, f32[4096]{0:T(1024)}, u32[]{:S(2)}) copy-start(f32[4096]{0:T(1024)} %param.12) | copy-start | bytes 49156
  7.2 121.1 %all-gather.5.cloned.1.call-start = ((), (), s32[]{:S(2)}) async-start(), calls=%async_computation.5 | async-start | bytes 8912896 | tf_op jit(solution)/shard_map/all_gather | solution.py:54
  8.0 180.9 %all-gather.3.cloned.1.call-start = ((), (), s32[]{:S(2)}) async-start(), calls=%async_computation.4 | async-start | bytes 9437184 | tf_op jit(solution)/shard_map/all_gather | solution.py:68
  10.4 4.2 copy-start.2
  17.2 187.2 %all-to-all-start.2 = ((bf16[8,2,256,32]{2,1,3,0:T(2,128)(2,1)}), bf16[8,2,256,32]{2,1,3,0:T(2,128)(2,1)S(1)}, u32[]{:S(2)}, u32[]{:S(2)}) async-start(bf16[8,2,256,32]{2,1,3,0:T(2,128)(2,1)} %broadcast_in_dim.4), calls=%async_computation.2 | async-start | bytes 524288 | tf_op jit(solution)/shard_map/all_to_all | solution.py:19
  46.7 142.2 %copy-start.7 = (f32[1024]{0:T(1024)S(1)}, f32[1024]{0:T(1024)}, u32[]{:S(2)}) copy-start(f32[1024]{0:T(1024)} %param.15) | copy-start | bytes 12292
  204.4 53.6 %all-to-all-start = ((bf16[8,2,2,256,256]{4,3,2,1,0:T(8,128)(2,1)}), bf16[8,2,2,256,256]{4,3,2,1,0:T(8,128)(2,1)}, u32[]{:S(2)}, u32[]{:S(2)}) async-start(bf16[8,2,2,256,256]{4,3,2,1,0:T(8,128)(2,1)} %fusion.12), calls=%async_computation | async-start | bytes 8388608 | tf_op jit(solution)/shard_map/all_to_all | solution.py:73
  257.9 24.8 %all-to-all-start.3 = ((bf16[1,16,1,256,32]{3,4,2,0,1:T(8,128)(2,1)}), bf16[1,16,1,256,32]{3,4,2,0,1:T(8,128)(2,1)S(1)}, u32[]{:S(2)}, u32[]{:S(2)}) async-start(bf16[1,16,1,256,32]{3,4,2,0,1:T(8,128)(2,1)} %bitcast.21), calls=%async_computation.3 | async-start | bytes 524288 | tf_op jit(solution)/shard_map/all_to_all | solution.py:78
  274.7 19.4 %copy-start.6 = (bf16[1,256]{1,0:T(2,128)(2,1)S(1)}, bf16[1,256]{1,0:T(2,128)(2,1)}, u32[]{:S(2)}) copy-start(bf16[1,256]{1,0:T(2,128)(2,1)} %param.18) | copy-start | bytes 1540
  274.7 20.1 %copy-start.8 = (bf16[1,128]{1,0:T(2,128)(2,1)S(1)}, bf16[1,128]{1,0:T(2,128)(2,1)}, u32[]{:S(2)}) copy-start(bf16[1,128]{1,0:T(2,128)(2,1)} %param.19) | copy-start | bytes 772
  282.7 193.1 %all-to-all-start.1 = ((bf16[2,16,1,256,256]{4,3,0,2,1:T(8,128)(2,1)}), bf16[2,16,1,256,256]{4,3,0,2,1:T(8,128)(2,1)}, u32[]{:S(2)}, u32[]{:S(2)}) async-start(bf16[2,16,1,256,256]{4,3,0,2,1:T(8,128)(2,1)} %copy.31), calls=%async_computation.1 | async-start | bytes 8388608 | tf_op jit(solution)/shard_map/all_to_all | solution.py:77
  295.6 191.9 %copy-start.4 = (bf16[4,8,16,256]{3,1,2,0:T(8,128)(2,1)}, bf16[4,8,16,256]{3,1,2,0:T(8,128)(2,1)S(1)}, u32[]{:S(2)}) copy-start(bf16[4,8,16,256]{3,1,2,0:T(8,128)(2,1)S(1)} %copy.43) | copy-start | bytes 786436
  479.7 1.3 copy-start.3
  488.0 8.7 %copy-start.1 = (bf16[4096,32]{0,1:T(8,128)(2,1)S(1)}, bf16[4096,32]{0,1:T(8,128)(2,1)}, u32[]{:S(2)}) copy-start(bf16[4096,32]{0,1:T(8,128)(2,1)} %param.14) | copy-start | bytes 786436
Sparse Core Ops, SparseCore 0:
  9.8 118.4 all-gather.4
  130.7 58.1 all-gather.2
